TPU v7x, 32 devices: a whole 2x2x4 slice. The times are simulated.
32 devices in a mesh: grp: 2 (over y), sp: 4 (over z), dp: 4 (over x, core).
Axes of the slice: x: 2, y: 2, z: 4, core: 2. Of those that a mesh axis runs over, the one named last changes fastest.
Arguments:
- gate_input: bfloat16 [8, 1536, 2048], P(('grp', 'dp'), 'sp'), parts along dimension 0, may hold values from -6 to 6
- value_input: bfloat16 [8, 1536, 2048], P(('grp', 'dp'), 'sp'), parts along dimension 0, may hold values from -6 to 6
- norm_gain: bfloat16 [2048], replicated, may hold values from 0.099609375 to 1.8984375
- norm_bias: bfloat16 [2048], replicated, may hold values from -2.5 to 2.5
- mix_weight: bfloat16 [16, 1024, 1024], P('sp', 'dp'), may hold values from -0.1875 to 0.1875
- mix_bias: bfloat16 [16, 1024], P('sp'), may hold values from 0.099609375 to 1.8984375
Outputs:
- gated: bfloat16 [8, 1536, 2048], P(('grp', 'dp'), 'sp'), parts along dimension 0
There are 2 independent parts, one for each index of `grp`. A program takes and returns all parts, laid end to end along the dimension named above; an argument that names none is the same for every part. Nothing has to cross between parts.
All inputs are finite; a program needn't handle non-finite values.
Results may differ from a plain program's by a relative error of at most 0.0053.
Values may be sent and summed in bfloat16 or wider, within the bound.
A program may use at most 64 MiB of HBM per device.

v0:
```python
import jax
import jax.numpy as jnp
from jax import lax
from jax.sharding import PartitionSpec as P

GD = 128
BLK = 1024


def mix_groups(normed_ex, mix_weight, mix_bias):
    seqs, length, local_width = normed_ex.shape
    groups_here = mix_weight.shape[0]
    nblocks = -(-length // BLK)
    padded = jnp.pad(normed_ex, ((0, 0), (0, nblocks * BLK - length), (0, 0)))
    blocks = padded.reshape(seqs * nblocks, BLK, groups_here, GD)
    piece = lax.all_gather(mix_weight, "dp", axis=1, tiled=True)
    count = piece.shape[1]
    rows = lax.iota(jnp.int32, count)
    cols = lax.iota(jnp.int32, BLK)
    keep = cols[None, :] <= rows[:, None]
    masked = jnp.where(keep[None], piece, jnp.zeros_like(piece))
    term = jnp.einsum("gts,bsgc->btgc", masked, blocks, preferred_element_type=jnp.float32)
    bias_rows = mix_bias.astype(jnp.float32)
    mixed = term + bias_rows.T[None, :, :, None]
    mixed = mixed.reshape(seqs, nblocks * BLK, local_width)[:, :length]
    return mixed.astype(jnp.bfloat16)


def body(gate_input, value_input, norm_gain, norm_bias, mix_weight, mix_bias):
    act = jax.nn.gelu(value_input.astype(jnp.float32))
    mean = jnp.mean(act, axis=-1, keepdims=True)
    var = jnp.mean(jnp.square(act - mean), axis=-1, keepdims=True)
    normed = (
        (act - mean) * lax.rsqrt(var + 1e-06) * norm_gain.astype(jnp.float32)
        + norm_bias.astype(jnp.float32)
    ).astype(jnp.bfloat16)
    normed_ex = lax.all_to_all(normed, "sp", split_axis=2, concat_axis=1, tiled=True)
    mixed = mix_groups(normed_ex, mix_weight, mix_bias)
    returned = lax.all_to_all(mixed, "sp", split_axis=1, concat_axis=2, tiled=True)
    gated = jax.nn.gelu(gate_input.astype(jnp.float32)) * returned.astype(jnp.float32)
    return gated.astype(jnp.bfloat16)


def solution(mesh):
    placed = (
        P(("grp", "dp"), "sp", None),
        P(("grp", "dp"), "sp", None),
        P(),
        P(),
        P("sp", "dp", None),
        P("sp", None),
    )
    return jax.shard_map(
        body, mesh=mesh, in_specs=placed, out_specs=P(("grp", "dp"), "sp", None), check_vma=False
    )
```

profile of v0, /device:TPU:0, one launch (start us, length us, event | category | flops | bytes accessed | tf_op | source)
XLA Modules:
  0.0 239.9 jit_solution(9603832664579578522)
XLA Ops:
  6.5 0.7 all-gather.2.cloned.1.call-update
  7.3 0.7 copy-done
  7.9 0.9 copy.17
  8.8 1.1 fusion.23
  10.0 1.3 multiply_reduce_fusion
  11.3 1.5 add_convert_fusion
  12.9 30.1 %copy.35 = bf16[1,384,2048]{1,0,2:T(2,128)(2,1)S(1)} copy(bf16[1,384,2048]{1,2,0:T(8,128)(2,1)S(1)} %add_convert_fusion) | data formatting | bytes 3145728 | tf_op jit(solution)/shard_map/convert_element_type | solution.py:36
  43.5 34.4 %reduce.2 = bf16[2048,384]{1,0:T(8,128)(2,1)} reduce(bf16[2048,1,384]{2,1,0:T(2,128)(2,1)S(1)} %bitcast.31, bf16[]{:T(256)} %broadcast.85), dimensions={1}, to_apply=%bitcast.30.reduce_sub_computation | reduce | bytes 3145730
  77.9 3.7 %reshape.69 = bf16[4,2,98304]{2,1,0:T(2,128)(2,1)} reshape(bf16[2048,384]{1,0:T(8,128)(2,1)} %reduce.2) | data formatting | bytes 3145728
  81.7 6.3 %all-to-all-start = ((bf16[4,2,98304]{2,1,0:T(2,128)(2,1)}), bf16[4,2,98304]{2,1,0:T(2,128)(2,1)}, u32[]{:S(2)}, u32[]{:S(2)}) async-start(bf16[4,2,98304]{2,1,0:T(2,128)(2,1)} %reshape.69), calls=%async_computation | async-start | bytes 3145728 | tf_op jit(solution)/shard_map/all_to_all | solution.py:37
  88.0 1.3 iota_compare_fusion
  89.3 35.8 %all-to-all-done = bf16[4,2,98304]{2,1,0:T(2,128)(2,1)} async-done(((bf16[4,2,98304]{2,1,0:T(2,128)(2,1)}), bf16[4,2,98304]{2,1,0:T(2,128)(2,1)}, u32[]{:S(2)}, u32[]{:S(2)}) %all-to-all-start) | async-done | bytes 1572896 | tf_op jit(solution)/shard_map/all_to_all | solution.py:37
  125.1 3.1 %reshape.70 = bf16[2048,1,384]{2,1,0:T(2,128)(2,1)S(1)} reshape(bf16[4,2,98304]{2,1,0:T(2,128)(2,1)} %all-to-all-done) | data formatting | bytes 3145728
  128.2 1.4 copy.27
  129.6 2.6 %copy.19 = bf16[1,4,384,512]{3,2,1,0:T(8,128)(2,1)} copy(bf16[1,4,384,512]{2,3,1,0:T(8,128)(2,1)} %bitcast.36) | data formatting | bytes 3145728 | tf_op jit(solution)/shard_map/all_to_all | solution.py:37
  132.2 1.6 pad.4
  133.8 2.1 reshape.64
  135.9 8.1 %fusion.4 = bf16[2,1024,4,128]{1,3,0,2:T(8,128)(2,1)} fusion(f32[1024,4]{0,1:T(4,128)S(1)} %convert_bitcast_fusion.1, bf16[4,1024,1024]{2,1,0:T(8,128)(2,1)} %all-gather.2.cloned.1.call-done, pred[1024,1024]{1,0:T(8,128)(4,1)S(1)} %copy-done.2, bf16[2,1024,4,128]{3,2,1,0:T(4,128)(2,1)} %reshape.64), kind=kOutput, calls=%fused_computation.13 | convolution fusion | flops 2153775104 | bytes 13647872 | tf_op jit(solution)/shard_map/gts,bsgc->btgc/dot_general | solution.py:22
  144.0 3.1 %copy.21 = bf16[2,1024,4,128]{3,2,1,0:T(4,128)(2,1)S(1)} copy(bf16[2,1024,4,128]{1,3,0,2:T(8,128)(2,1)} %fusion.4) | data formatting | bytes 4194304 | tf_op jit(solution)/shard_map/convert.5
  147.2 2.2 reshape.65
  149.4 1.4 slice-done
  150.8 11.7 %copy.34 = bf16[1,1536,512]{2,0,1:T(2,128)(2,1)S(1)} copy(bf16[1,1536,512]{2,1,0:T(8,128)(2,1)S(1)} %slice-done) | data formatting | bytes 3145728 | tf_op jit(solution)/shard_map/slice | solution.py:25
  162.5 11.1 %reduce.3 = bf16[1536,512]{1,0:T(8,128)(2,1)} reduce(bf16[1536,1,512]{2,1,0:T(2,128)(2,1)S(1)} %bitcast.32, bf16[]{:T(256)} %broadcast.85), dimensions={1}, to_apply=%bitcast.29.reduce_sub_computation | reduce | bytes 3145730
  173.5 4.3 %reshape.71 = bf16[4,2,98304]{2,1,0:T(2,128)(2,1)} reshape(bf16[1536,512]{1,0:T(8,128)(2,1)} %reduce.3) | data formatting | bytes 3145728
  177.8 4.3 %all-to-all-start.1 = ((bf16[4,2,98304]{2,1,0:T(2,128)(2,1)}), bf16[4,2,98304]{2,1,0:T(2,128)(2,1)}, u32[]{:S(2)}, u32[]{:S(2)}) async-start(bf16[4,2,98304]{2,1,0:T(2,128)(2,1)} %reshape.71), calls=%async_computation.1 | async-start | bytes 3145728 | tf_op jit(solution)/shard_map/all_to_all | solution.py:39
  182.2 1.6 copy.16
  183.7 35.0 %all-to-all-done.1 = bf16[4,2,98304]{2,1,0:T(2,128)(2,1)} async-done(((bf16[4,2,98304]{2,1,0:T(2,128)(2,1)}), bf16[4,2,98304]{2,1,0:T(2,128)(2,1)}, u32[]{:S(2)}, u32[]{:S(2)}) %all-to-all-start.1) | async-done | bytes 1572896 | tf_op jit(solution)/shard_map/all_to_all | solution.py:39
  218.7 3.1 %reshape.72 = bf16[1536,1,512]{2,1,0:T(2,128)(2,1)S(1)} reshape(bf16[4,2,98304]{2,1,0:T(2,128)(2,1)} %all-to-all-done.1) | data formatting | bytes 3145728
  222.2 2.1 convert_bitcast_fusion
  224.3 2.4 copy.24
  226.7 3.8 %fusion.12 = bf16[1,384,2048]{1,2,0:T(8,128)(2,1)} fusion(bf16[1,384,2048]{1,2,0:T(8,128)(2,1)} %copy.16, f32[1,384,4,512]{1,3,2,0:T(8,128)S(1)} %copy.24), kind=kLoop, calls=%fused_computation.22 | loop fusion | flops 8650752 | bytes 6291456 | tf_op jit(solution)/shard_map/convert_element_type | solution.py:41
  230.5 2.6 %copy.25 = bf16[1,384,2048]{2,1,0:T(8,128)(2,1)} copy(bf16[1,384,2048]{1,2,0:T(8,128)(2,1)} %fusion.12) | data formatting | bytes 3145728 | tf_op jit(solution)/shard_map/convert_element_type | solution.py:41
  (21 shorter events, 1.0 us)
Async XLA Ops:
  6.5 1.4 copy-start
  6.5 2.3 copy-start.4
  6.5 2.3 copy-start.5
  6.5 129.4 %all-gather.2.cloned.1.call-start = ((), (), s32[]{:S(2)}) async-start(), calls=%async_computation.2 | async-start | bytes 10485760 | tf_op jit(solution)/shard_map/all_gather | solution.py:16
  77.9 11.4 %copy-start.3 = (bf16[4,1024]{1,0:T(4,128)(2,1)S(1)}, bf16[4,1024]{1,0:T(4,128)(2,1)}, u32[]{:S(2)}) copy-start(bf16[4,1024]{1,0:T(4,128)(2,1)} %param.11) | copy-start | bytes 24580
  81.7 43.4 %all-to-all-start = ((bf16[4,2,98304]{2,1,0:T(2,128)(2,1)}), bf16[4,2,98304]{2,1,0:T(2,128)(2,1)}, u32[]{:S(2)}, u32[]{:S(2)}) async-start(bf16[4,2,98304]{2,1,0:T(2,128)(2,1)} %reshape.69), calls=%async_computation | async-start | bytes 3145728 | tf_op jit(solution)/shard_map/all_to_all | solution.py:37
  132.2 3.7 %copy-start.2 = (pred[1024,1024]{1,0:T(8,128)(4,1)S(1)}, pred[1024,1024]{1,0:T(8,128)(4,1)}, u32[]{:S(2)}) copy-start(pred[1024,1024]{1,0:T(8,128)(4,1)} %iota_compare_fusion) | copy-start | bytes 3145732
  149.4 1.4 slice-start
  173.5 8.6 %copy-start.1 = (bf16[1,384,2048]{2,1,0:T(8,128)(2,1)S(1)}, bf16[1,384,2048]{2,1,0:T(8,128)(2,1)}, u32[]{:S(2)}) copy-start(bf16[1,384,2048]{2,1,0:T(8,128)(2,1)} %param.6) | copy-start | bytes 4718596
  177.8 40.9 %all-to-all-start.1 = ((bf16[4,2,98304]{2,1,0:T(2,128)(2,1)}), bf16[4,2,98304]{2,1,0:T(2,128)(2,1)}, u32[]{:S(2)}, u32[]{:S(2)}) async-start(bf16[4,2,98304]{2,1,0:T(2,128)(2,1)} %reshape.71), calls=%async_computation.1 | async-start | bytes 3145728 | tf_op jit(solution)/shard_map/all_to_all | solution.py:39
Sparse Core Ops, SparseCore 0:
  8.9 60.9 all-gather.1
where the time goes:
time: 241 us; the launch traced here: 240 us
  local copies, waits for them, and re-layouts  79.4 us (33%)
  waiting for transfers between devices  71.5 us (30%)
  other arithmetic  56.7 us (24%)
  between operations  13.5 us (6%)
  starting transfers between devices  10.7 us (4%)
  matrix products  8.09 us (3%)
    unnamed x2, other arithmetic  45.5 us
    all_to_all x1, waiting for transfers between devices, body(): lax.all_to_all(normed, 'sp', split_axis=2, concat_axis=1, tiled=True)  35.8 us
    all_to_all x1, waiting for transfers between devices, body(): lax.all_to_all(mixed, 'sp', split_axis=1, concat_axis=2, tiled=True)  35 us
    convert_element_type x1, local copies, waits for them, and re-layouts, body(): normed = ((act - mean) * lax.rsqrt(var + 1e-06) * norm_gain.astype(jnp.fl...  30.1 us
    unnamed x20, local copies, waits for them, and re-layouts  19.2 us
    slice x3, local copies, waits for them, and re-layouts, mix_groups(): mixed = mixed.reshape(seqs, nblocks * BLK, local_width)[:, :length]  13.1 us
    dot_general x1, matrix products, mix_groups(): jnp.einsum('gts,bsgc->btgc', masked, blocks, preferred_element_type=jnp.f...  8.09 us
    all_to_all x1, starting transfers between devices, body(): lax.all_to_all(normed, 'sp', split_axis=2, concat_axis=1, tiled=True)  6.35 us
  transfers between devices with their start and end apart: 3, of which 2 were waited for; matrix products, arithmetic and copies ran while one was open for 36% of the time, Pallas kernels for 0%

commit v1 on v0

--- a/solution.py
+++ b/solution.py
@@ -5,6 +5,18 @@
 
 GD = 128
 BLK = 1024
+
+
+def guide_files(a0, mesh_name):
+    return jnp.concatenate(
+        lax.all_to_all(
+            jnp.stack(jnp.split(a0, lax.axis_size(mesh_name), axis=2), axis=0),
+            axis_name=mesh_name,
+            split_axis=0,
+            concat_axis=0,
+        ),
+        axis=1,
+    )
 
 
 def mix_groups(normed_ex, mix_weight, mix_bias):
@@ -34,7 +46,7 @@
         (act - mean) * lax.rsqrt(var + 1e-06) * norm_gain.astype(jnp.float32)
         + norm_bias.astype(jnp.float32)
     ).astype(jnp.bfloat16)
-    normed_ex = lax.all_to_all(normed, "sp", split_axis=2, concat_axis=1, tiled=True)
+    normed_ex = guide_files(normed, "sp")
     mixed = mix_groups(normed_ex, mix_weight, mix_bias)
     returned = lax.all_to_all(mixed, "sp", split_axis=1, concat_axis=2, tiled=True)
     gated = jax.nn.gelu(gate_input.astype(jnp.float32)) * returned.astype(jnp.float32)

time: 241 us -> 176 us (0.73)
  local copies, waits for them, and re-layouts: 79.4 us -> 41.3 us
  other arithmetic: 56.7 us -> 21.5 us
  waiting for transfers between devices: 71.5 us -> 80.1 us
    unnamed x2 -> x1, other arithmetic: 45.5 us -> 11 us
    convert_element_type x1 -> x0, local copies, waits for them, and re-layouts: 30.1 us -> none  [body(): normed = ((act - mean) * lax.rsqrt(var + 1e-06) * norm_gain.astype(jnp.fl...]
    unnamed x20 -> x17, local copies, waits for them, and re-layouts: 19.2 us -> 12.1 us
    all_gather x1, waiting for transfers between devices: 0.01 us -> 6.87 us  [mix_groups(): piece = lax.all_gather(mix_weight, 'dp', axis=1, tiled=True)]
    all_to_all x1 -> x0, local copies, waits for them, and re-layouts: 2.64 us -> none  [body(): lax.all_to_all(normed, 'sp', split_axis=2, concat_axis=1, tiled=True)]
    another operation x1 -> x3, local copies, waits for them, and re-layouts: 3.13 us -> 4.92 us
  transfers between devices with their start and end apart: 3 -> 3, of which waited for: 2 -> 3; matrix products, arithmetic and copies ran while one was open for 36% -> 7% of each run, Pallas kernels for 0% -> 0%
where the time goes in v1:
time: 176 us; the launch traced here: 175 us
  waiting for transfers between devices  80.1 us (46%)
  local copies, waits for them, and re-layouts  41.3 us (23%)
  other arithmetic  21.5 us (12%)
  between operations  13.5 us (8%)
  starting transfers between devices  10.9 us (6%)
  matrix products  8.1 us (5%)
    all_to_all x1, waiting for transfers between devices, guide_files(): lax.all_to_all(jnp.stack(jnp.split(a0, lax.axis_size(mesh_name), axis=2),...  36.6 us
    all_to_all x1, waiting for transfers between devices, body(): lax.all_to_all(mixed, 'sp', split_axis=1, concat_axis=2, tiled=True)  35.9 us
    slice x3, local copies, waits for them, and re-layouts, mix_groups(): mixed = mixed.reshape(seqs, nblocks * BLK, local_width)[:, :length]  13.1 us
    unnamed x17, local copies, waits for them, and re-layouts  12.1 us
    unnamed x1, other arithmetic  11 us
    dot_general x1, matrix products, mix_groups(): jnp.einsum('gts,bsgc->btgc', masked, blocks, preferred_element_type=jnp.f...  8.1 us
    all_gather x1, waiting for transfers between devices, mix_groups(): piece = lax.all_gather(mix_weight, 'dp', axis=1, tiled=True)  6.87 us
    all_to_all x1, starting transfers between devices, guide_files(): lax.all_to_all(jnp.stack(jnp.split(a0, lax.axis_size(mesh_name), axis=2),...  6.35 us
  transfers between devices with their start and end apart: 3, of which 3 were waited for; matrix products, arithmetic and copies ran while one was open for 7% of the time, Pallas kernels for 0%

profile of v1, /device:TPU:0, one launch (start us, length us, event | category | flops | bytes accessed | tf_op | source)
XLA Modules:
  0.0 175.5 jit_solution(3552523051469836391)
XLA Ops:
  6.5 0.7 all-gather.2.cloned.1.call-update
  7.3 0.7 copy-done.1
  7.9 0.9 copy.23
  8.8 1.1 fusion.23
  10.0 1.3 multiply_reduce_fusion
  11.3 1.5 add_convert_fusion
  13.1 0.2 pad_maximum_fusion
  13.3 1.6 copy.24
  15.0 6.3 %all-to-all-start = ((bf16[4,1,384,512]{3,2,1,0:T(8,128)(2,1)}), bf16[4,1,384,512]{3,2,1,0:T(8,128)(2,1)S(1)}, u32[]{:S(2)}, u32[]{:S(2)}) async-start(bf16[4,1,384,512]{3,2,1,0:T(8,128)(2,1)} %copy.24), calls=%async_computation | async-start | bytes 3145728 | tf_op jit(solution)/shard_map/all_to_all | solution.py:12
  21.3 0.3 iota_compare_fusion
  21.6 36.6 %all-to-all-done = bf16[4,1,384,512]{3,2,1,0:T(8,128)(2,1)S(1)} async-done(((bf16[4,1,384,512]{3,2,1,0:T(8,128)(2,1)}), bf16[4,1,384,512]{3,2,1,0:T(8,128)(2,1)S(1)}, u32[]{:S(2)}, u32[]{:S(2)}) %all-to-all-start) | async-done | bytes 1572896 | tf_op jit(solution)/shard_map/all_to_all | solution.py:12
  58.3 1.1 copy-done
  59.4 1.5 pad.4
  61.0 2.1 %reshape.68 = bf16[2,1024,4,128]{3,2,1,0:T(4,128)(2,1)} reshape(bf16[1,2048,512]{2,1,0:T(8,128)(2,1)S(1)} %pad.4) | data formatting | bytes 4194304 | tf_op jit(solution)/shard_map/reshape | solution.py:27
  63.0 6.9 %all-gather.2.cloned.1.call-done = bf16[4,1024,1024]{2,1,0:T(8,128)(2,1)} async-done(((bf16[4,256,1024]{2,1,0:T(8,128)(2,1)}), bf16[4,1024,1024]{2,1,0:T(8,128)(2,1)}) %all-gather.2.cloned.1.call-update) | async-done | bytes 8388624 | tf_op jit(solution)/shard_map/all_gather | solution.py:28
  69.9 8.1 %fusion.4 = bf16[2,1024,4,128]{1,3,0,2:T(8,128)(2,1)} fusion(f32[1024,4]{0,1:T(4,128)S(1)} %convert_bitcast_fusion.1, bf16[4,1024,1024]{2,1,0:T(8,128)(2,1)} %all-gather.2.cloned.1.call-done, pred[1024,1024]{1,0:T(8,128)(4,1)S(1)} %iota_compare_fusion, bf16[2,1024,4,128]{3,2,1,0:T(4,128)(2,1)} %reshape.68), kind=kOutput, calls=%fused_computation.13 | convolution fusion | flops 2153775104 | bytes 13647872 | tf_op jit(solution)/shard_map/gts,bsgc->btgc/dot_general | solution.py:34
  78.0 3.1 %copy.26 = bf16[2,1024,4,128]{3,2,1,0:T(4,128)(2,1)S(1)} copy(bf16[2,1024,4,128]{1,3,0,2:T(8,128)(2,1)} %fusion.4) | data formatting | bytes 4194304 | tf_op jit(solution)/shard_map/convert.5
  81.2 2.2 %reshape.69 = bf16[1,2048,512]{2,1,0:T(8,128)(2,1)} reshape(bf16[2,1024,4,128]{3,2,1,0:T(4,128)(2,1)S(1)} %copy.26) | data formatting | bytes 4194304 | tf_op jit(solution)/shard_map/reshape | solution.py:37
  83.4 1.4 slice-done
  84.8 11.7 %copy.37 = bf16[1,1536,512]{2,0,1:T(2,128)(2,1)S(1)} copy(bf16[1,1536,512]{2,1,0:T(8,128)(2,1)S(1)} %slice-done) | data formatting | bytes 3145728 | tf_op jit(solution)/shard_map/slice | solution.py:37
  96.5 0.5 broadcast.85
  97.0 11.0 %reduce.2 = bf16[1536,512]{1,0:T(8,128)(2,1)} reduce(bf16[1536,1,512]{2,1,0:T(2,128)(2,1)S(1)} %bitcast.32, bf16[]{:T(256)} %broadcast.85), dimensions={1}, to_apply=%bitcast.31.reduce_sub_computation | reduce | bytes 3145730
  108.0 4.2 %reshape.73 = bf16[4,2,98304]{2,1,0:T(2,128)(2,1)} reshape(bf16[1536,512]{1,0:T(8,128)(2,1)} %reduce.2) | data formatting | bytes 3145728
  112.2 4.6 %all-to-all-start.1 = ((bf16[4,2,98304]{2,1,0:T(2,128)(2,1)}), bf16[4,2,98304]{2,1,0:T(2,128)(2,1)}, u32[]{:S(2)}, u32[]{:S(2)}) async-start(bf16[4,2,98304]{2,1,0:T(2,128)(2,1)} %reshape.73), calls=%async_computation.1 | async-start | bytes 3145728 | tf_op jit(solution)/shard_map/all_to_all | solution.py:51
  116.8 1.6 copy.22
  118.4 35.9 %all-to-all-done.1 = bf16[4,2,98304]{2,1,0:T(2,128)(2,1)} async-done(((bf16[4,2,98304]{2,1,0:T(2,128)(2,1)}), bf16[4,2,98304]{2,1,0:T(2,128)(2,1)}, u32[]{:S(2)}, u32[]{:S(2)}) %all-to-all-start.1) | async-done | bytes 1572896 | tf_op jit(solution)/shard_map/all_to_all | solution.py:51
  154.3 3.1 %reshape.74 = bf16[1536,1,512]{2,1,0:T(2,128)(2,1)S(1)} reshape(bf16[4,2,98304]{2,1,0:T(2,128)(2,1)} %all-to-all-done.1) | data formatting | bytes 3145728
  157.4 0.4 copy.28
  157.8 2.1 %convert_bitcast_fusion = f32[1,384,4,512]{3,1,2,0:T(8,128)} fusion(bf16[1,4,384,512]{3,2,1,0:T(8,128)(2,1)S(1)} %bitcast.35), kind=kLoop, calls=%fused_computation.28 | loop fusion | flops 786432 | bytes 4718592 | tf_op jit(solution)/shard_map/convert_element_type | solution.py:52
  159.9 2.4 %copy.29 = f32[1,384,4,512]{1,3,2,0:T(8,128)S(1)} copy(f32[1,384,4,512]{3,1,2,0:T(8,128)} %convert_bitcast_fusion) | data formatting | bytes 6291456 | tf_op jit(solution)/shard_map/convert_element_type | solution.py:52
  162.3 3.8 %fusion.12 = bf16[1,384,2048]{1,2,0:T(8,128)(2,1)} fusion(bf16[1,384,2048]{1,2,0:T(8,128)(2,1)} %copy.22, f32[1,384,4,512]{1,3,2,0:T(8,128)S(1)} %copy.29), kind=kLoop, calls=%fused_computation.22 | loop fusion | flops 8650752 | bytes 6291456 | tf_op jit(solution)/shard_map/convert_element_type | solution.py:53
  166.0 2.6 %copy.30 = bf16[1,384,2048]{2,1,0:T(8,128)(2,1)} copy(bf16[1,384,2048]{1,2,0:T(8,128)(2,1)} %fusion.12) | data formatting | bytes 3145728 | tf_op jit(solution)/shard_map/convert_element_type | solution.py:53
  (18 shorter events, 0.2 us)
Async XLA Ops:
  6.5 1.4 copy-start.1
  6.5 2.3 %copy-start.4 = (bf16[2048]{0:T(1024)(128)(2,1)S(1)}, bf16[2048]{0:T(1024)(128)(2,1)}, u32[]{:S(2)}) copy-start(bf16[2048]{0:T(1024)(128)(2,1)} %param.8) | copy-start | bytes 12292
  6.5 2.3 %copy-start.5 = (bf16[2048]{0:T(1024)(128)(2,1)S(1)}, bf16[2048]{0:T(1024)(128)(2,1)}, u32[]{:S(2)}) copy-start(bf16[2048]{0:T(1024)(128)(2,1)} %param.9) | copy-start | bytes 12292
  6.5 63.4 %all-gather.2.cloned.1.call-start = ((), (), s32[]{:S(2)}) async-start(), calls=%async_computation.2 | async-start | bytes 10485760 | tf_op jit(solution)/shard_map/all_gather | solution.py:28
  13.3 8.3 %copy-start.3 = (bf16[4,1024]{1,0:T(4,128)(2,1)S(1)}, bf16[4,1024]{1,0:T(4,128)(2,1)}, u32[]{:S(2)}) copy-start(bf16[4,1024]{1,0:T(4,128)(2,1)} %param.11) | copy-start | bytes 24580
  15.0 43.3 %all-to-all-start = ((bf16[4,1,384,512]{3,2,1,0:T(8,128)(2,1)}), bf16[4,1,384,512]{3,2,1,0:T(8,128)(2,1)S(1)}, u32[]{:S(2)}, u32[]{:S(2)}) async-start(bf16[4,1,384,512]{3,2,1,0:T(8,128)(2,1)} %copy.24), calls=%async_computation | async-start | bytes 3145728 | tf_op jit(solution)/shard_map/all_to_all | solution.py:12
  58.3 1.1 copy-start
  83.4 1.4 slice-start
  108.0 8.8 %copy-start.2 = (bf16[1,384,2048]{2,1,0:T(8,128)(2,1)S(1)}, bf16[1,384,2048]{2,1,0:T(8,128)(2,1)}, u32[]{:S(2)}) copy-start(bf16[1,384,2048]{2,1,0:T(8,128)(2,1)} %param.6) | copy-start | bytes 4718596
  112.2 42.1 %all-to-all-start.1 = ((bf16[4,2,98304]{2,1,0:T(2,128)(2,1)}), bf16[4,2,98304]{2,1,0:T(2,128)(2,1)}, u32[]{:S(2)}, u32[]{:S(2)}) async-start(bf16[4,2,98304]{2,1,0:T(2,128)(2,1)} %reshape.73), calls=%async_computation.1 | async-start | bytes 3145728 | tf_op jit(solution)/shard_map/all_to_all | solution.py:51
Sparse Core Ops, SparseCore 0:
  8.9 60.9 all-gather.1
